TPU v7x, 32 devices: a whole 2x2x4 slice. The times are simulated.
32 devices in a mesh: sp: 8 (over z, y), tp: 4 (over x, core).
Axes of the slice: x: 2, y: 2, z: 4, core: 2. Of those that a mesh axis runs over, the one named last changes fastest.
Arguments:
- arriving_hidden_sum: bfloat16 [8192, 2048], P('sp'), may hold values from -40 to 40
- content_entries_clustered: bfloat16 [8192, 4096], P('sp', 'tp'), may hold values from -6 to 6
- leaving_switch_entries: bfloat16 [8192, 4096], P('sp', 'tp'), may hold values from -6 to 6
- linked_source_target_pairs: bfloat16 [8192, 8, 2, 128], P('sp', 'tp'), may hold values from -1.78125 to 1.78125
- raw_interval_length: bfloat16 [8192, 64], P('sp', 'tp'), may hold values from -5 to 5
- spike_extra_lognoise: float32 [8192, 64], P('sp', 'tp'), may hold values from -0.6 to 0
- content_filter_kernel: bfloat16 [4, 4096], P(None, 'tp'), may hold values from -3 to 3
- coupling_filter_kernel: bfloat16 [4, 8, 2, 128], P(None, 'tp'), may hold values from -3 to 3
- interval_shift_vector: float32 [64], P('tp'), may hold values from -0.5 to 0.5
- fading_speed_exponent: float32 [64], P('tp'), may hold values from -16 to -2.9
- skip_channel_factor: float32 [64], P('tp'), may hold values from 1 to 10
- cluster_rescale_vector: float32 [4096], P('tp'), may hold values from 0.1 to 1.9
- blender_final_tensor: bfloat16 [4096, 2048], P('tp'), may hold values from -0.09375 to 0.09375
- prelayer_rescale_vector: float32 [2048], replicated, may hold values from 0.1 to 1.9
- switching_linear_tensor: bfloat16 [2048, 5632], P('sp', 'tp'), may hold values from -0.125 to 0.125
- widening_linear_tensor: bfloat16 [2048, 5632], P('sp', 'tp'), may hold values from -0.125 to 0.125
- contracting_linear_tensor: bfloat16 [5632, 2048], P('tp', 'sp'), may hold values from -0.078125 to 0.078125
Outputs:
- residual_out: bfloat16 [8192, 2048], P('sp', 'tp')
All inputs are finite; a program needn't handle non-finite values.
Results may differ from a plain program's by a relative error of at most 0.012.
Values may be sent and summed in bfloat16 or wider, within the bound.
A program may use at most 128 MiB of HBM per device.

v0:
```python
import jax
import jax.numpy as jnp
from jax import lax
from jax.sharding import PartitionSpec as P

D = 2048
BLOCK_POSITIONS = 128
EPS = 1e-06
highest = lax.Precision.HIGHEST


def from_behind(block, axis, distance):
    devices = range(lax.axis_size(axis))
    route = [(i - distance, i) for i in devices if i - distance in devices]
    return lax.ppermute(block, axis, route)


def prefix(array, axis, combine, identity):
    count, place = (lax.axis_size(axis), lax.axis_index(axis))
    everything = jax.tree.map(
        lambda part, kind: lax.all_gather(part.astype(kind), axis),
        array,
        (jnp.bfloat16, jnp.bfloat16),
    )
    start = jax.tree.map(
        lambda part, zero: jnp.broadcast_to(jnp.asarray(zero, part.dtype), part.shape),
        array,
        identity,
    )

    def lap(k, before):
        reached = k < place
        new = combine(
            before, jax.tree.map(lambda part, own: part[k].astype(own.dtype), everything, array)
        )
        return jax.tree.map(lambda a, b: jnp.where(reached, a, b), new, before)

    return lax.fori_loop(0, count, lap, start)


def conv_block(values, rims, taps):
    taps_count = taps.shape[0]
    length = values.shape[0]
    padded = jnp.concatenate([rims, values], axis=0).astype(jnp.float32)
    running = jnp.zeros(values.shape, jnp.float32)
    for tap_index in range(taps_count):
        running = running + padded[tap_index : tap_index + length] * taps[tap_index].astype(
            jnp.float32
        )
    return jax.nn.silu(running).astype(jnp.bfloat16)


def combine_states(former, latter):
    return (former[0] * jnp.exp(latter[1])[:, :, None, None] + latter[0], former[1] + latter[1])


def shards(
    arriving_hidden_sum,
    content_entries_clustered,
    leaving_switch_entries,
    linked_source_target_pairs,
    raw_interval_length,
    spike_extra_lognoise,
    content_filter_kernel,
    coupling_filter_kernel,
    interval_shift_vector,
    fading_speed_exponent,
    skip_channel_factor,
    cluster_rescale_vector,
    blender_final_tensor,
    prelayer_rescale_vector,
    switching_linear_tensor,
    widening_linear_tensor,
    contracting_linear_tensor,
):
    length = content_entries_clustered.shape[0]
    heads_per_device = raw_interval_length.shape[1]
    groups_dev = linked_source_target_pairs.shape[1]
    per_group = heads_per_device // groups_dev
    head_size = content_entries_clustered.shape[1] // heads_per_device
    state_size = linked_source_target_pairs.shape[3]
    taps_count = content_filter_kernel.shape[0]
    block_count = length // BLOCK_POSITIONS
    couple_flat = linked_source_target_pairs.reshape(length, -1)
    value_rims, couple_rims = from_behind(
        (
            content_entries_clustered[length - taps_count + 1 :],
            couple_flat[length - taps_count + 1 :],
        ),
        "sp",
        1,
    )
    values = conv_block(content_entries_clustered, value_rims, content_filter_kernel)
    coupled = conv_block(
        couple_flat, couple_rims, coupling_filter_kernel.reshape(taps_count, -1)
    ).reshape(length, groups_dev, 2, state_size)
    value_blocks = values.reshape(block_count, BLOCK_POSITIONS, heads_per_device, head_size)
    write_maps = coupled[:, :, 0].reshape(block_count, BLOCK_POSITIONS, groups_dev, state_size)
    read_maps = coupled[:, :, 1].reshape(block_count, BLOCK_POSITIONS, groups_dev, state_size)
    interval_lengths = jax.nn.softplus(
        raw_interval_length.astype(jnp.float32) + interval_shift_vector
    )
    fading_log_factor = (
        -jnp.exp(fading_speed_exponent) * interval_lengths + spike_extra_lognoise
    ).reshape(block_count, BLOCK_POSITIONS, heads_per_device)
    interval_lengths = interval_lengths.reshape(block_count, BLOCK_POSITIONS, heads_per_device)
    cum_log = jnp.cumsum(fading_log_factor, axis=1)
    head_cum = jnp.swapaxes(cum_log, 1, 2)
    log_gap = head_cum[:, :, :, None] - head_cum[:, :, None, :]
    causal = jnp.tril(jnp.ones((BLOCK_POSITIONS, BLOCK_POSITIONS), bool))
    intersection = jnp.einsum(
        "blgn,bsgn->bgls", read_maps, write_maps, preferred_element_type=jnp.float32
    )
    intersection = jnp.repeat(intersection, per_group, axis=1)
    weights = (
        intersection
        * jnp.exp(jnp.where(causal, log_gap, -jnp.inf))
        * jnp.swapaxes(interval_lengths, 1, 2)[:, :, None, :]
    ).astype(jnp.bfloat16)
    within = jnp.einsum(
        "bhls,bshp->blhp", weights, value_blocks, preferred_element_type=jnp.float32
    )
    end_log = cum_log[:, -1]
    scaled = (
        value_blocks * (interval_lengths * jnp.exp(end_log[:, None, :] - cum_log))[..., None]
    ).astype(jnp.bfloat16)
    block_states = jnp.einsum(
        "blgn,blgrp->bgrpn",
        write_maps,
        scaled.reshape(block_count, BLOCK_POSITIONS, groups_dev, per_group, head_size),
        preferred_element_type=jnp.float32,
    )
    end_grouped = end_log.reshape(block_count, groups_dev, per_group)

    def carry_step(carry_state, inputs):
        block_added, block_end = inputs
        return (carry_state * jnp.exp(block_end)[:, :, None, None] + block_added, carry_state)

    zeros_state = jnp.zeros((groups_dev, per_group, head_size, state_size), jnp.float32)
    final_state, entering = lax.scan(carry_step, zeros_state, (block_states, end_grouped))
    read_wide = read_maps.astype(jnp.float32)
    carried = (
        jnp.einsum("blgn,bgrpn->blgrp", read_wide, entering, precision=highest).reshape(
            block_count, BLOCK_POSITIONS, heads_per_device, head_size
        )
        * jnp.exp(cum_log)[..., None]
    )
    device_log = jnp.sum(end_log, axis=0).reshape(groups_dev, per_group)
    incoming, _ = prefix(
        (final_state, device_log), "sp", combine_states, (zeros_state, jnp.zeros_like(device_log))
    )
    prior_log = jnp.cumsum(end_log, axis=0) - end_log
    reach_decay = jnp.exp(cum_log + prior_log[:, None, :])
    arrived = (
        jnp.einsum("blgn,grpn->blgrp", read_wide, incoming, precision=highest).reshape(
            block_count, BLOCK_POSITIONS, heads_per_device, head_size
        )
        * reach_decay[..., None]
    )
    mixer = (within + carried + arrived).reshape(
        length, heads_per_device, head_size
    ) + values.reshape(length, heads_per_device, head_size).astype(
        jnp.float32
    ) * skip_channel_factor[
        None, :, None
    ]
    gated = mixer.reshape(length, heads_per_device * head_size) * jax.nn.silu(
        leaving_switch_entries.astype(jnp.float32)
    )
    grouped = gated.reshape(length, groups_dev, per_group * head_size)
    grouped = grouped * lax.rsqrt(jnp.mean(grouped * grouped, axis=-1, keepdims=True) + EPS)
    mixed_rows = (
        grouped.reshape(length, heads_per_device * head_size) * cluster_rescale_vector
    ).astype(jnp.bfloat16)
    partial_sum = jnp.dot(mixed_rows, blender_final_tensor, preferred_element_type=jnp.float32)
    rounded = lax.optimization_barrier(partial_sum.astype(jnp.bfloat16)).astype(jnp.float32)
    col_count = D // lax.axis_size("tp")
    offset = lax.axis_index("tp") * col_count
    mixer_cols = lax.psum_scatter(
        rounded.astype(jnp.bfloat16), "tp", scatter_dimension=1, tiled=True
    ).astype(jnp.float32)
    resid_cols = lax.dynamic_slice_in_dim(arriving_hidden_sum, offset, col_count, 1)
    residual_mid = (resid_cols.astype(jnp.float32) + mixer_cols).astype(jnp.bfloat16)
    squares = residual_mid.astype(jnp.float32)
    square_sums = lax.psum(jnp.sum(squares * squares, axis=1), "tp")
    gain_cols = lax.dynamic_slice_in_dim(prelayer_rescale_vector, offset, col_count, 0)
    normed_cols = (squares * lax.rsqrt(square_sums / D + EPS)[:, None] * gain_cols).astype(
        jnp.bfloat16
    )
    normed = lax.all_gather(normed_cols, "tp", axis=1, tiled=True)
    gate_pre = jnp.dot(
        normed,
        lax.all_gather(switching_linear_tensor, "sp", axis=0, tiled=True),
        preferred_element_type=jnp.float32,
    )
    up_pre = jnp.dot(
        normed,
        lax.all_gather(widening_linear_tensor, "sp", axis=0, tiled=True),
        preferred_element_type=jnp.float32,
    )
    hidden = (jax.nn.silu(gate_pre) * up_pre).astype(jnp.bfloat16)
    down_terms = jnp.dot(
        hidden,
        lax.all_gather(contracting_linear_tensor, "sp", axis=1, tiled=True),
        preferred_element_type=jnp.float32,
    )
    down_rounded = lax.optimization_barrier(down_terms.astype(jnp.bfloat16)).astype(jnp.float32)
    mlp_cols = lax.psum_scatter(
        down_rounded.astype(jnp.bfloat16), "tp", scatter_dimension=1, tiled=True
    ).astype(jnp.float32)
    return (residual_mid.astype(jnp.float32) + 0.5 * mlp_cols).astype(jnp.bfloat16)


def solution(mesh):
    placed = (
        P("sp", None),
        P("sp", "tp"),
        P("sp", "tp"),
        P("sp", "tp", None, None),
        P("sp", "tp"),
        P("sp", "tp"),
        P(None, "tp"),
        P(None, "tp", None, None),
        P("tp"),
        P("tp"),
        P("tp"),
        P("tp"),
        P("tp", None),
        P(),
        P("sp", "tp"),
        P("sp", "tp"),
        P("tp", "sp"),
    )
    return jax.shard_map(
        shards, mesh=mesh, in_specs=placed, out_specs=P("sp", "tp"), check_vma=False
    )
```

profile of v0, /device:TPU:0, one launch (start us, length us, event | category | flops | bytes accessed | tf_op | source)
XLA Modules:
  0.0 612.9 jit_solution(5842465863375640701)
XLA Ops:
  8.2 4.9 collective-permute-start
  14.6 4.1 collective-permute-start.1
  20.6 23.3 %fusion.43 = f32[8,128,16]{2,0,1:T(8,128)S(1)} fusion(f32[8,128,16]{2,0,1:T(8,128)S(1)} %copy.81), kind=kOutput, calls=%fused_computation.88 | output fusion | flops 2080768 | bytes 131072 | tf_op jit(solution)/shard_map/jit(cumsum)/reduce_window_sum | solution.py:107
  44.3 1.5 slice_convert_fusion.3
  45.8 1.3 fusion.42
  47.2 2.9 copy.74
  50.0 3.7 copy.76
  53.7 1.2 convert.10
  54.9 1.2 convert.11
  56.1 1.3 convert.12
  57.4 1.2 convert.13
  58.6 1.8 maximum_convert_fusion.1
  60.4 3.0 multiply_convert_fusion.5
  63.4 1.1 fusion.40
  64.5 2.0 copy.78
  66.6 1.2 maximum_convert_fusion
  67.9 4.5 convert_bitcast_fusion
  74.4 2.7 fusion.25
  77.1 16.2 %while.27 = (s32[]{:T(128)}, f32[2,8,64,128]{3,2,1,0:T(8,128)S(1)}, f32[8,2,8,64,128]{4,3,2,1,0:T(8,128)}, f32[8,2,8]{2,1,0:T(2,128)S(1)}, f32[8,2,8,64,128]{4,3,2,1,0:T(8,128)}, /*index=5*/s32[]{:T(128)}, s32[]{:T(128)}) while((s32[]{:T(128)}, f32[2,8,64,128]{3,2,1,0:T(8,128)S(1)}, f32[8,2,8,64,128]{4,3,2,1,0:T(8,128)}, ...), condition=%wide.region_2.3_spmd.clone, body=%wide.region_1.2_spmd.clone.sunk | while | flops 524291 | bytes 2622240 | solution.py:140
  77.9 1.2 bitcast_add_fusion.3
  80.0 1.2 bitcast_add_fusion.3
  82.0 1.2 bitcast_add_fusion.3
  84.0 1.2 bitcast_add_fusion.3
  86.0 1.2 bitcast_add_fusion.3
  88.1 1.2 bitcast_add_fusion.3
  90.1 1.2 bitcast_add_fusion.3
  92.1 1.2 bitcast_add_fusion.3
  94.3 1.1 fusion.41
  95.4 1.2 copy.92
  96.6 1.2 copy.94
  98.1 4.0 copy.96
  102.2 17.5 %all_gather.22 = bf16[8,2,8]{2,1,0:T(2,128)(2,1)S(1)} all-gather(bf16[1,2,8]{2,1,0:T(2,128)(2,1)S(1)} %convert_element_type.180), channel_id=1, replica_groups=mesh['sp'=8,'tp'=4] {'sp'}, dimensions={0}, use_global_device_ids=true | all-gather | bytes 288 | tf_op jit(solution)/shard_map/all_gather | solution.py:21
  119.7 1.3 copy.77
  121.0 2.6 fusion.34
  123.6 2.0 copy.106
  125.7 3.5 fusion.31
  129.1 13.8 %all-gather.15.cloned.1.call-done = bf16[16,8,64,128]{3,2,1,0:T(8,128)(2,1)} async-done(((bf16[2,8,64,128]{3,2,1,0:T(8,128)(2,1)}), bf16[16,8,64,128]{3,2,1,0:T(8,128)(2,1)}) %all-gather.15.cloned.1.call-update) | async-done | bytes 2097168 | tf_op jit(solution)/shard_map/all_gather | solution.py:21
  143.0 9.0 %while.28 = (s32[]{:T(128)}, f32[2,8,64,128]{3,2,1,0:T(8,128)S(1)}, s32[]{:T(128)}, bf16[8,2,8]{2,1,0:T(2,128)(2,1)S(1)}, bf16[8,2,8,64,128]{4,3,2,1,0:T(8,128)(2,1)}, /*index=5*/s32[]{:T(128)}, s32[]{:T(128)}) while((s32[]{:T(128)}, f32[2,8,64,128]{3,2,1,0:T(8,128)S(1)}, s32[]{:T(128)}, bf16[8,2,8]{2,1,0:T(2,128)(2,1)S(1)}, ...), condition=%wide.region_5.6_spmd.clone, body=%wide.region_4.5_spmd.clone.sunk | while | flops 655380 | bytes 1310985 | solution.py:38
  143.0 1.1 fusion.65
  144.1 1.1 fusion.65
  145.2 1.1 fusion.65
  146.4 1.1 fusion.65
  147.5 1.1 fusion.65
  148.6 1.1 fusion.65
  149.8 1.1 fusion.65
  152.0 1.8 convolution_bitcast_fusion
  156.1 1.1 copy-done
  157.9 6.0 fusion.12
  164.0 5.6 copy.95
  169.6 2.8 bitcast_reduce_fusion
  172.9 1.7 copy-done.11
  174.6 6.2 %convolution_convert_fusion.1 = bf16[1024,2048]{1,0:T(8,128)(2,1)} fusion(bf16[1024,1024]{0,1:T(8,128)(2,1)S(1)} %fusion.11, bf16[1024,2048]{1,0:T(8,128)(2,1)S(1)} %copy-done.11), kind=kOutput, calls=%fused_computation.39 | convolution fusion | flops 4297064448 | bytes 10485760 | tf_op jit(solution)/shard_map/dot_general | solution.py:175
  182.6 41.3 %reduce-scatter.3.cloned.1.call-done = bf16[1024,512]{1,0:T(8,128)(2,1)} async-done(((bf16[1024,2048]{1,0:T(8,128)(2,1)}), bf16[1024,512]{1,0:T(8,128)(2,1)}) %reduce-scatter.3.cloned.1.call-update) | async-done | bytes 1048592 | tf_op jit(solution)/shard_map/reduce_scatter | solution.py:179
  224.0 2.0 fusion.18
  226.0 5.8 psum.7
  231.7 1.3 fusion.20
  234.2 84.3 %all-gather.9.cloned.1.call-done = bf16[2048,1408]{1,0:T(8,128)(2,1)} async-done(((bf16[256,1408]{1,0:T(8,128)(2,1)}), bf16[2048,1408]{1,0:T(8,128)(2,1)}) %all-gather.9.cloned.1.call-update) | async-done | bytes 5767184 | tf_op jit(solution)/shard_map/all_gather | solution.py:193
  318.5 34.1 %all-gather.7.cloned.1.call-done = bf16[1024,2048]{1,0:T(8,128)(2,1)} async-done(((bf16[1024,512]{1,0:T(8,128)(2,1)}), bf16[1024,2048]{1,0:T(8,128)(2,1)}) %all-gather.7.cloned.1.call-update) | async-done | bytes 4194320 | tf_op jit(solution)/shard_map/all_gather | solution.py:190
  352.6 11.7 %fusion.44 = f32[1024,1408]{1,0:T(8,128)} fusion(bf16[1024,2048]{1,0:T(8,128)(2,1)} %all-gather.7.cloned.1.call-done, bf16[2048,1408]{1,0:T(8,128)(2,1)} %all-gather.9.cloned.1.call-done), kind=kOutput, calls=%fused_computation.89 | convolution fusion | flops 5905580032 | bytes 15728640 | tf_op jit(solution)/shard_map/dot_general | solution.py:191
  364.3 82.7 %all-gather.11.cloned.1.call-done = bf16[2048,1408]{1,0:T(8,128)(2,1)} async-done(((bf16[256,1408]{1,0:T(8,128)(2,1)}), bf16[2048,1408]{1,0:T(8,128)(2,1)}) %all-gather.11.cloned.1.call-update) | async-done | bytes 5767184 | tf_op jit(solution)/shard_map/all_gather | solution.py:198
  447.0 93.2 %all-gather.13.cloned.1.call-done = bf16[1408,2048]{1,0:T(8,128)(2,1)} async-done(((bf16[1408,256]{1,0:T(8,128)(2,1)}), bf16[1408,2048]{1,0:T(8,128)(2,1)}) %all-gather.13.cloned.1.call-update) | async-done | bytes 5767184 | tf_op jit(solution)/shard_map/all_gather | solution.py:204
  540.2 20.5 %convolution_convert_fusion = bf16[1024,2048]{1,0:T(8,128)(2,1)} fusion(bf16[1408,2048]{1,0:T(8,128)(2,1)} %all-gather.13.cloned.1.call-done, f32[1024,1408]{1,0:T(8,128)} %fusion.44, bf16[1024,2048]{1,0:T(8,128)(2,1)} %all-gather.7.cloned.1.call-done, bf16[2048,1408]{1,0:T(8,128)(2,1)} %all-gather.11.cloned.1.call-done), kind=kOutput, calls=%fused_computation.38 | convolution fusion | flops 11821907968 | bytes 25690112 | tf_op jit(solution)/shard_map/dot_general | solution.py:202
  560.8 42.7 %reduce-scatter.5.cloned.1.call-done = bf16[1024,512]{1,0:T(8,128)(2,1)} async-done(((bf16[1024,2048]{1,0:T(8,128)(2,1)}), bf16[1024,512]{1,0:T(8,128)(2,1)}) %reduce-scatter.5.cloned.1.call-update) | async-done | bytes 1048592 | tf_op jit(solution)/shard_map/reduce_scatter | solution.py:208
  603.5 2.5 fusion.21
  (97 shorter events, 23.2 us)
Async XLA Ops:
  6.5 136.4 %all-gather.15.cloned.1.call-start = ((), (), s32[]{:S(2)}) async-start(), calls=%async_computation.8 | async-start | bytes 2359296 | tf_op jit(solution)/shard_map/all_gather | solution.py:21
  8.2 58.4 %collective-permute-start = (bf16[3,1024]{0,1:T(8,128)(2,1)}, bf16[3,1024]{0,1:T(8,128)(2,1)S(1)}, u32[]{:S(2)}, u32[]{:S(2)}) collective-permute-start(bf16[3,1024]{0,1:T(8,128)(2,1)} %copy.73), channel_id=1, source_target_pairs={{0,4},{4,8},{8,12},{12,16},{16,20},{20,24},{24,28},{1,5},{5,9},{9,... | collective-permute-start | bytes 18440 | tf_op jit(solution)/shard_map/ppermute | solution.py:15
  14.6 44.0 %collective-permute-start.1 = (bf16[3,512]{0,1:T(8,128)(2,1)}, bf16[3,512]{0,1:T(8,128)(2,1)}, u32[]{:S(2)}, u32[]{:S(2)}) collective-permute-start(bf16[3,512]{0,1:T(8,128)(2,1)} %bitcast.4), channel_id=1, source_target_pairs={{0,4},{4,8},{8,12},{12,16},{16,20},{20,24},{24,28},{1,5},{5,9},{9,... | collective-permute-start | bytes 9224 | tf_op jit(solution)/shard_map/ppermute | solution.py:15
  66.6 1.2 copy-start.6
  66.6 1.2 copy-start.7
  66.6 1.3 copy-start.8
  73.3 1.0 copy-start.3
  94.1 8.0 %copy-start.10 = (f32[16]{0:T(128)S(1)}, f32[16]{0:T(128)}, u32[]{:S(2)}) copy-start(f32[16]{0:T(128)} %param.31) | copy-start | bytes 196
  94.1 129.9 %reduce-scatter.3.cloned.1.call-start = ((), (), s32[]{:S(2)}) async-start(), calls=%async_computation.2 | async-start | bytes 5242880 | tf_op jit(solution)/shard_map/reduce_scatter | solution.py:179
  121.0 4.7 copy-start.5
  153.8 1.2 copy-start.4
  155.1 2.2 copy-start
  155.1 2.9 copy-start.2
  164.0 5.6 copy-start.1
  169.6 2.9 copy-start.9
  172.4 2.2 copy-start.11
  180.9 137.6 %all-gather.9.cloned.1.call-start = ((), (), s32[]{:S(2)}) async-start(), calls=%async_computation.4 | async-start | bytes 6488064 | tf_op jit(solution)/shard_map/all_gather | solution.py:193
  181.6 171.0 %all-gather.7.cloned.1.call-start = ((), (), s32[]{:S(2)}) async-start(), calls=%async_computation.3 | async-start | bytes 5242880 | tf_op jit(solution)/shard_map/all_gather | solution.py:190
  233.0 213.9 %all-gather.11.cloned.1.call-start = ((), (), s32[]{:S(2)}) async-start(), calls=%async_computation.5 | async-start | bytes 6488064 | tf_op jit(solution)/shard_map/all_gather | solution.py:198
  233.6 306.6 %all-gather.13.cloned.1.call-start = ((), (), s32[]{:S(2)}) async-start(), calls=%async_computation.6 | async-start | bytes 6488064 | tf_op jit(solution)/shard_map/all_gather | solution.py:204
  234.2 369.3 %reduce-scatter.5.cloned.1.call-start = ((), (), s32[]{:S(2)}) async-start(), calls=%async_computation.7 | async-start | bytes 5242880 | tf_op jit(solution)/shard_map/reduce_scatter | solution.py:208
Sparse Core Ops, SparseCore 0:
  94.2 48.7 all-gather.14
  181.0 42.9 reduce-scatter.2
  226.2 92.2 all-gather.8
  319.9 32.6 all-gather.6
  354.6 92.3 all-gather.10
  448.9 91.2 all-gather.12
  560.9 42.5 reduce-scatter.4
where the time goes:
time: 615 us; the launch traced here: 613 us
  waiting for transfers between devices  394 us (64%)
  other arithmetic  78.2 us (13%)
  matrix products  55.1 us (9%)
  local copies, waits for them, and re-layouts  38.7 us (6%)
  blocking collectives  23.2 us (4%)
  between operations  13.8 us (2%)
  starting transfers between devices  9.44 us (2%)
    all_gather x1, waiting for transfers between devices, shards(): lax.all_gather(contracting_linear_tensor, 'sp', axis=1, tiled=True)  93.2 us
    all_gather x1, waiting for transfers between devices, shards(): lax.all_gather(switching_linear_tensor, 'sp', axis=0, tiled=True)  84.3 us
    all_gather x1, waiting for transfers between devices, shards(): lax.all_gather(widening_linear_tensor, 'sp', axis=0, tiled=True)  82.7 us
    reduce_scatter x1, waiting for transfers between devices, shards(): lax.psum_scatter(down_rounded.astype(jnp.bfloat16), 'tp', scatter_dimensi...  42.7 us
    reduce_scatter x1, waiting for transfers between devices, shards(): lax.psum_scatter(rounded.astype(jnp.bfloat16), 'tp', scatter_dimension=1,...  41.3 us
    all_gather x1, waiting for transfers between devices, shards(): normed = lax.all_gather(normed_cols, 'tp', axis=1, tiled=True)  34.1 us
    another operation x1, other arithmetic, shards(): cum_log = jnp.cumsum(fading_log_factor, axis=1)  23.3 us
    dot_general x1, matrix products, shards(): jnp.dot(hidden, lax.all_gather(contracting_linear_tensor, 'sp', axis=1, t...  20.5 us
  transfers between devices with their start and end apart: 9, of which 7 were waited for; matrix products, arithmetic and copies ran while one was open for 13% of the time, Pallas kernels for 0%

commit v1 on v0

--- a/solution.py
+++ b/solution.py
@@ -187,7 +187,12 @@
     normed_cols = (squares * lax.rsqrt(square_sums / D + EPS)[:, None] * gain_cols).astype(
         jnp.bfloat16
     )
-    normed = lax.all_gather(normed_cols, "tp", axis=1, tiled=True)
+    ring = [normed_cols]
+    for hop in range(3):
+        ring.append(lax.ppermute(ring[-1], "tp", [(dev, (dev + 1) % 4) for dev in range(4)]))
+    normed = jnp.roll(
+        jnp.concatenate(ring[::-1], axis=1), (lax.axis_index("tp") + 1) * ring[0].shape[1], axis=1
+    )
     gate_pre = jnp.dot(
         normed,
         lax.all_gather(switching_linear_tensor, "sp", axis=0, tiled=True),

time: 615 us -> 579 us (0.941)
  waiting for transfers between devices: 394 us -> 347 us
  local copies, waits for them, and re-layouts: 38.7 us -> 48 us
    all_gather x1, waiting for transfers between devices: 84.3 us -> 31.7 us  [shards(): lax.all_gather(switching_linear_tensor, 'sp', axis=0, tiled=True)]
    ppermute x0 -> x3, waiting for transfers between devices: none -> 42.8 us  [shards(): lax.ppermute(ring[-1], 'tp', [(dev, (dev + 1) % 4) for dev in range(4)])]
    all_gather x1 -> x0, waiting for transfers between devices: 34.1 us -> none  [shards(): normed = lax.all_gather(normed_cols, 'tp', axis=1, tiled=True)]
    all_gather x1, waiting for transfers between devices: 93.2 us -> 81.5 us  [shards(): lax.all_gather(contracting_linear_tensor, 'sp', axis=1, tiled=True)]
    all_gather x1, waiting for transfers between devices: 82.7 us -> 92.6 us  [shards(): lax.all_gather(widening_linear_tensor, 'sp', axis=0, tiled=True)]
    unnamed x31 -> x37, local copies, waits for them, and re-layouts: 18.3 us -> 27.5 us
  transfers between devices with their start and end apart: 9 -> 11, of which waited for: 7 -> 9; matrix products, arithmetic and copies ran while one was open for 13% -> 16% of each run, Pallas kernels for 0% -> 0%
where the time goes in v1:
time: 579 us; the launch traced here: 577 us
  waiting for transfers between devices  347 us (60%)
  other arithmetic  79.9 us (14%)
  matrix products  55.2 us (10%)
  local copies, waits for them, and re-layouts  48 us (8%)
  blocking collectives  23.2 us (4%)
  between operations  13.8 us (2%)
  starting transfers between devices  9.46 us (2%)
    all_gather x1, waiting for transfers between devices, shards(): lax.all_gather(widening_linear_tensor, 'sp', axis=0, tiled=True)  92.6 us
    all_gather x1, waiting for transfers between devices, shards(): lax.all_gather(contracting_linear_tensor, 'sp', axis=1, tiled=True)  81.5 us
    ppermute x3, waiting for transfers between devices, shards(): lax.ppermute(ring[-1], 'tp', [(dev, (dev + 1) % 4) for dev in range(4)])  42.8 us
    reduce_scatter x1, waiting for transfers between devices, shards(): lax.psum_scatter(down_rounded.astype(jnp.bfloat16), 'tp', scatter_dimensi...  42.7 us
    reduce_scatter x1, waiting for transfers between devices, shards(): lax.psum_scatter(rounded.astype(jnp.bfloat16), 'tp', scatter_dimension=1,...  40.4 us
    all_gather x1, waiting for transfers between devices, shards(): lax.all_gather(switching_linear_tensor, 'sp', axis=0, tiled=True)  31.7 us
    unnamed x37, local copies, waits for them, and re-layouts  27.5 us
    another operation x1, other arithmetic, shards(): cum_log = jnp.cumsum(fading_log_factor, axis=1)  23.3 us
  transfers between devices with their start and end apart: 11, of which 9 were waited for; matrix products, arithmetic and copies ran while one was open for 16% of the time, Pallas kernels for 0%

profile of v1, /device:TPU:0, one launch (start us, length us, event | category | flops | bytes accessed | tf_op | source)
XLA Modules:
  0.0 577.0 jit_solution(13001684687960305276)
XLA Ops:
  8.2 4.9 collective-permute-start
  14.6 4.1 collective-permute-start.1
  20.6 23.3 %fusion.51 = f32[8,128,16]{2,0,1:T(8,128)S(1)} fusion(f32[8,128,16]{2,0,1:T(8,128)S(1)} %copy.81), kind=kOutput, calls=%fused_computation.102 | output fusion | flops 2080768 | bytes 131072 | tf_op jit(solution)/shard_map/jit(cumsum)/reduce_window_sum | solution.py:107
  44.3 1.5 slice_convert_fusion.3
  45.8 1.3 fusion.50
  47.2 2.9 copy.74
  50.0 3.7 copy.76
  53.7 1.2 convert.10
  54.9 1.2 convert.11
  56.1 1.3 convert.12
  57.4 1.2 convert.13
  58.6 1.8 maximum_convert_fusion.1
  60.4 3.0 multiply_convert_fusion.5
  64.5 2.0 copy.78
  66.6 1.2 maximum_convert_fusion
  67.9 4.5 convert_bitcast_fusion
  74.4 2.7 fusion.31
  77.1 16.2 %while.27 = (s32[]{:T(128)}, f32[2,8,64,128]{3,2,1,0:T(8,128)S(1)}, f32[8,2,8,64,128]{4,3,2,1,0:T(8,128)}, f32[8,2,8]{2,1,0:T(2,128)S(1)}, f32[8,2,8,64,128]{4,3,2,1,0:T(8,128)}, /*index=5*/s32[]{:T(128)}, s32[]{:T(128)}) while((s32[]{:T(128)}, f32[2,8,64,128]{3,2,1,0:T(8,128)S(1)}, f32[8,2,8,64,128]{4,3,2,1,0:T(8,128)}, ...), condition=%wide.region_2.3_spmd.clone, body=%wide.region_1.2_spmd.clone.sunk | while | flops 524291 | bytes 2622240 | solution.py:140
  77.9 1.2 bitcast_add_fusion.3
  80.0 1.2 bitcast_add_fusion.3
  82.0 1.2 bitcast_add_fusion.3
  84.0 1.2 bitcast_add_fusion.3
  86.0 1.2 bitcast_add_fusion.3
  88.1 1.2 bitcast_add_fusion.3
  90.1 1.2 bitcast_add_fusion.3
  92.1 1.2 bitcast_add_fusion.3
  95.4 1.2 copy.92
  96.6 1.2 copy.94
  98.1 4.0 copy.96
  102.2 17.5 %all_gather.19 = bf16[8,2,8]{2,1,0:T(2,128)(2,1)S(1)} all-gather(bf16[1,2,8]{2,1,0:T(2,128)(2,1)S(1)} %convert_element_type.180), channel_id=1, replica_groups=mesh['sp'=8,'tp'=4] {'sp'}, dimensions={0}, use_global_device_ids=true | all-gather | bytes 288 | tf_op jit(solution)/shard_map/all_gather | solution.py:21
  119.7 1.3 copy.77
  121.0 2.6 fusion.40
  123.6 2.0 copy.106
  125.7 3.5 fusion.37
  129.1 13.8 %all-gather.12.cloned.1.call-done = bf16[16,8,64,128]{3,2,1,0:T(8,128)(2,1)} async-done(((bf16[2,8,64,128]{3,2,1,0:T(8,128)(2,1)}), bf16[16,8,64,128]{3,2,1,0:T(8,128)(2,1)}) %all-gather.12.cloned.1.call-update) | async-done | bytes 2097168 | tf_op jit(solution)/shard_map/all_gather | solution.py:21
  143.0 9.0 %while.28 = (s32[]{:T(128)}, f32[2,8,64,128]{3,2,1,0:T(8,128)S(1)}, s32[]{:T(128)}, bf16[8,2,8]{2,1,0:T(2,128)(2,1)S(1)}, bf16[8,2,8,64,128]{4,3,2,1,0:T(8,128)(2,1)}, /*index=5*/s32[]{:T(128)}, s32[]{:T(128)}) while((s32[]{:T(128)}, f32[2,8,64,128]{3,2,1,0:T(8,128)S(1)}, s32[]{:T(128)}, bf16[8,2,8]{2,1,0:T(2,128)(2,1)S(1)}, ...), condition=%wide.region_5.6_spmd.clone, body=%wide.region_4.5_spmd.clone.sunk | while | flops 655380 | bytes 1310985 | solution.py:38
  152.0 1.8 convolution_bitcast_fusion
  156.1 1.1 copy-done
  157.9 6.0 %fusion.12 = f32[8,128,16,64]{1,3,2,0:T(8,128)} fusion(f32[8,128,16,64]{1,3,2,0:T(8,128)S(1)} %bitcast.129, f32[8,128,16,64]{1,3,2,0:T(8,128)S(1)} %bitcast.128, f32[8,128,16]{1,2,0:T(8,128)S(1)} %copy.94, f32[8,128,16]{1,2,0:T(8,128)S(1)} %copy.92, f32[8,16,128,128]{3,2,1,0:T(8,128)S(1)} %bitcast.126, f32[8,16,128]{2,1,0:T(8,128)S(1)} %copy.84, ...), kind=kOutput, calls=%fused_computation.30 | convolution fusion | flops 283115520 | bytes 23347200 | tf_op jit(solution)/shard_map/bhls,bshp->blhp/dot_general | solution.py:120
  164.0 5.6 copy.95
  169.6 2.8 bitcast_reduce_fusion
  172.9 1.7 copy-done.11
  174.6 6.2 %convolution_convert_fusion.1 = bf16[1024,2048]{1,0:T(8,128)(2,1)} fusion(bf16[1024,1024]{0,1:T(8,128)(2,1)S(1)} %fusion.11, bf16[1024,2048]{1,0:T(8,128)(2,1)S(1)} %copy-done.11), kind=kOutput, calls=%fused_computation.39 | convolution fusion | flops 4297064448 | bytes 10485760 | tf_op jit(solution)/shard_map/dot_general | solution.py:175
  183.5 40.4 %reduce-scatter.3.cloned.1.call-done = bf16[1024,512]{1,0:T(8,128)(2,1)} async-done(((bf16[1024,2048]{1,0:T(8,128)(2,1)}), bf16[1024,512]{1,0:T(8,128)(2,1)}) %reduce-scatter.3.cloned.1.call-update) | async-done | bytes 1048592 | tf_op jit(solution)/shard_map/reduce_scatter | solution.py:179
  223.9 2.0 fusion.24
  225.9 5.8 psum.7
  232.1 14.2 %collective-permute-done.2 = bf16[1024,512]{1,0:T(8,128)(2,1)S(1)} collective-permute-done((bf16[1024,512]{1,0:T(8,128)(2,1)S(1)}, bf16[1024,512]{1,0:T(8,128)(2,1)S(1)}, u32[]{:S(2)}, u32[]{:S(2)}) %collective-permute-start.2) | collective-permute-done | bytes 1048608 | tf_op jit(solution)/shard_map/ppermute | solution.py:192
  246.3 14.2 %collective-permute-done.3 = bf16[1024,512]{1,0:T(8,128)(2,1)S(1)} collective-permute-done((bf16[1024,512]{1,0:T(8,128)(2,1)S(1)}, bf16[1024,512]{1,0:T(8,128)(2,1)S(1)}, u32[]{:S(2)}, u32[]{:S(2)}) %collective-permute-start.3) | collective-permute-done | bytes 1048608 | tf_op jit(solution)/shard_map/ppermute | solution.py:192
  260.5 14.3 %collective-permute-done.4 = bf16[1024,512]{1,0:T(8,128)(2,1)} collective-permute-done((bf16[1024,512]{1,0:T(8,128)(2,1)S(1)}, bf16[1024,512]{1,0:T(8,128)(2,1)}, u32[]{:S(2)}, u32[]{:S(2)}) %collective-permute-start.4) | collective-permute-done | bytes 1048608 | tf_op jit(solution)/shard_map/ppermute | solution.py:192
  274.8 2.3 constant_dynamic-update-slice_fusion.7
  277.2 1.1 constant_dynamic-update-slice_fusion.6
  278.3 1.1 constant_dynamic-update-slice_fusion.5
  279.4 1.4 constant_dynamic-update-slice_fusion.4
  280.8 2.3 constant_dynamic-update-slice_fusion.3
  283.2 1.2 constant_dynamic-update-slice_fusion.2
  284.3 1.1 constant_dynamic-update-slice_fusion.1
  285.5 1.3 constant_dynamic-update-slice_fusion
  286.8 31.7 %all-gather.6.cloned.1.call-done = bf16[2048,1408]{1,0:T(8,128)(2,1)} async-done(((bf16[256,1408]{1,0:T(8,128)(2,1)}), bf16[2048,1408]{1,0:T(8,128)(2,1)}) %all-gather.6.cloned.1.call-update) | async-done | bytes 5767184 | tf_op jit(solution)/shard_map/all_gather | solution.py:198
  318.5 11.7 %fusion.20 = f32[1024,1408]{1,0:T(8,128)} fusion(bf16[2048,1408]{1,0:T(8,128)(2,1)} %all-gather.6.cloned.1.call-done, bf16[1024,4096]{1,0:T(8,128)(2,1)} %constant_dynamic-update-slice_fusion, s32[]{:T(128)S(6)} %select_n.53), kind=kOutput, calls=%fused_computation.42 | convolution fusion | flops 5905580032 | bytes 15728644 | tf_op jit(solution)/shard_map/dot_general | solution.py:196
  330.2 81.5 %all-gather.10.cloned.1.call-done = bf16[1408,2048]{1,0:T(8,128)(2,1)} async-done(((bf16[1408,256]{1,0:T(8,128)(2,1)}), bf16[1408,2048]{1,0:T(8,128)(2,1)}) %all-gather.10.cloned.1.call-update) | async-done | bytes 5767184 | tf_op jit(solution)/shard_map/all_gather | solution.py:209
  411.7 92.6 %all-gather.8.cloned.1.call-done = bf16[2048,1408]{1,0:T(8,128)(2,1)} async-done(((bf16[256,1408]{1,0:T(8,128)(2,1)}), bf16[2048,1408]{1,0:T(8,128)(2,1)}) %all-gather.8.cloned.1.call-update) | async-done | bytes 5767184 | tf_op jit(solution)/shard_map/all_gather | solution.py:203
  504.3 20.6 %convolution_convert_fusion = bf16[1024,2048]{1,0:T(8,128)(2,1)} fusion(bf16[1408,2048]{1,0:T(8,128)(2,1)} %all-gather.10.cloned.1.call-done, f32[1024,1408]{1,0:T(8,128)} %fusion.20, bf16[2048,1408]{1,0:T(8,128)(2,1)} %all-gather.8.cloned.1.call-done, bf16[1024,4096]{1,0:T(8,128)(2,1)} %constant_dynamic-update-slice_fusion, s32[]{:T(128)S(6)} %select_n.53), kind=kOutput, calls=%fused_computation.38 | convolution fusion | flops 11821907968 | bytes 25690116 | tf_op jit(solution)/shard_map/dot_general | solution.py:207
  524.9 42.7 %reduce-scatter.5.cloned.1.call-done = bf16[1024,512]{1,0:T(8,128)(2,1)} async-done(((bf16[1024,2048]{1,0:T(8,128)(2,1)}), bf16[1024,512]{1,0:T(8,128)(2,1)}) %reduce-scatter.5.cloned.1.call-update) | async-done | bytes 1048592 | tf_op jit(solution)/shard_map/reduce_scatter | solution.py:213
  567.6 2.5 fusion.27
  (108 shorter events, 33.1 us)
Async XLA Ops:
  6.5 136.4 %all-gather.12.cloned.1.call-start = ((), (), s32[]{:S(2)}) async-start(), calls=%async_computation.7 | async-start | bytes 2359296 | tf_op jit(solution)/shard_map/all_gather | solution.py:21
  8.2 58.4 %collective-permute-start = (bf16[3,1024]{0,1:T(8,128)(2,1)}, bf16[3,1024]{0,1:T(8,128)(2,1)S(1)}, u32[]{:S(2)}, u32[]{:S(2)}) collective-permute-start(bf16[3,1024]{0,1:T(8,128)(2,1)} %copy.73), channel_id=1, source_target_pairs={{0,4},{4,8},{8,12},{12,16},{16,20},{20,24},{24,28},{1,5},{5,9},{9,... | collective-permute-start | bytes 18440 | tf_op jit(solution)/shard_map/ppermute | solution.py:15
  14.6 44.0 %collective-permute-start.1 = (bf16[3,512]{0,1:T(8,128)(2,1)}, bf16[3,512]{0,1:T(8,128)(2,1)}, u32[]{:S(2)}, u32[]{:S(2)}) collective-permute-start(bf16[3,512]{0,1:T(8,128)(2,1)} %bitcast.4), channel_id=1, source_target_pairs={{0,4},{4,8},{8,12},{12,16},{16,20},{20,24},{24,28},{1,5},{5,9},{9,... | collective-permute-start | bytes 9224 | tf_op jit(solution)/shard_map/ppermute | solution.py:15
  66.6 1.2 copy-start.6
  66.6 1.2 copy-start.7
  66.6 1.3 copy-start.8
  73.3 1.0 copy-start.3
  94.1 8.0 %copy-start.10 = (f32[16]{0:T(128)S(1)}, f32[16]{0:T(128)}, u32[]{:S(2)}) copy-start(f32[16]{0:T(128)} %param.31) | copy-start | bytes 196
  94.1 129.8 %reduce-scatter.3.cloned.1.call-start = ((), (), s32[]{:S(2)}) async-start(), calls=%async_computation.2 | async-start | bytes 5242880 | tf_op jit(solution)/shard_map/reduce_scatter | solution.py:179
  121.0 4.7 copy-start.5
  153.8 1.2 copy-start.4
  155.1 2.2 copy-start
  155.1 2.9 copy-start.2
  164.0 5.6 copy-start.1
  169.6 2.9 copy-start.9
  172.4 2.2 copy-start.11
  180.8 137.6 %all-gather.6.cloned.1.call-start = ((), (), s32[]{:S(2)}) async-start(), calls=%async_computation.3 | async-start | bytes 6488064 | tf_op jit(solution)/shard_map/all_gather | solution.py:198
  181.6 230.1 %all-gather.10.cloned.1.call-start = ((), (), s32[]{:S(2)}) async-start(), calls=%async_computation.5 | async-start | bytes 6488064 | tf_op jit(solution)/shard_map/all_gather | solution.py:209
  182.1 322.1 %all-gather.8.cloned.1.call-start = ((), (), s32[]{:S(2)}) async-start(), calls=%async_computation.4 | async-start | bytes 6488064 | tf_op jit(solution)/shard_map/all_gather | solution.py:203
  182.7 384.9 %reduce-scatter.5.cloned.1.call-start = ((), (), s32[]{:S(2)}) async-start(), calls=%async_computation.6 | async-start | bytes 5242880 | tf_op jit(solution)/shard_map/reduce_scatter | solution.py:213
  232.0 14.3 %collective-permute-start.2 = (bf16[1024,512]{1,0:T(8,128)(2,1)S(1)}, bf16[1024,512]{1,0:T(8,128)(2,1)S(1)}, u32[]{:S(2)}, u32[]{:S(2)}) collective-permute-start(bf16[1024,512]{1,0:T(8,128)(2,1)S(1)} %fusion.26), channel_id=1, source_target_pairs={{0,1},{1,2},{2,3},{3,0},{4,5},{5,6},{6,7},{7,4},{8,9},{9,10},{10,1... | collective-permute-start | bytes 3145736 | tf_op jit(solution)/shard_map/ppermute | solution.py:192
  246.3 14.2 %collective-permute-start.3 = (bf16[1024,512]{1,0:T(8,128)(2,1)S(1)}, bf16[1024,512]{1,0:T(8,128)(2,1)S(1)}, u32[]{:S(2)}, u32[]{:S(2)}) collective-permute-start(bf16[1024,512]{1,0:T(8,128)(2,1)S(1)} %collective-permute-done.2), channel_id=1, source_target_pairs={{0,1},{1,2},{2,3},{3,0},{4,5},{5,6},{6,7},{7,4},{8,9},{9,10},{10,1... | collective-permute-start | bytes 3145736 | tf_op jit(solution)/shard_map/ppermute | solution.py:192
  260.5 14.3 %collective-permute-start.4 = (bf16[1024,512]{1,0:T(8,128)(2,1)S(1)}, bf16[1024,512]{1,0:T(8,128)(2,1)}, u32[]{:S(2)}, u32[]{:S(2)}) collective-permute-start(bf16[1024,512]{1,0:T(8,128)(2,1)S(1)} %collective-permute-done.3), channel_id=1, source_target_pairs={{0,1},{1,2},{2,3},{3,0},{4,5},{5,6},{6,7},{7,4},{8,9},{9,10},{10,1... | collective-permute-start | bytes 3145736 | tf_op jit(solution)/shard_map/ppermute | solution.py:192
Sparse Core Ops, SparseCore 0:
  94.2 48.7 all-gather.11
  180.9 42.9 reduce-scatter.2
  226.1 92.2 all-gather.5
  320.4 91.3 all-gather.9
  413.7 90.4 all-gather.7
  525.0 42.5 reduce-scatter.4
